TPU v7x, 32 devices: a whole 2x2x4 slice. The times are simulated.
32 devices in a mesh: fs: 8 (over z, core), tp: 4 (over y, x).
Axes of the slice: x: 2, y: 2, z: 4, core: 2. Of those that a mesh axis runs over, the one named last changes fastest.
Arguments:
- rows_later: bfloat16 [6144, 2048], P('fs'), may hold values from -6 to 6
- rows_earlier: bfloat16 [6144, 2048], P('fs'), may hold values from -6 to 6
- out_cotangent: bfloat16 [6144, 4096], P('fs', 'tp'), may hold values from -6 to 6
- gate_proj: bfloat16 [2048, 4096], P('fs', 'tp'), may hold values from -0.125 to 0.125
- up_proj: bfloat16 [2048, 4096], P('fs', 'tp'), may hold values from -0.125 to 0.125
- conv_taps: float32 [3, 4096], P(None, 'tp'), may hold values from -4 to 4
- conv_bias: float32 [4096], P('tp'), may hold values from -3 to 3
- gate_grad_sum: float32 [2048, 4096], P('fs', 'tp'), may hold values from -6 to 6
- up_grad_sum: float32 [2048, 4096], P('fs', 'tp'), may hold values from -6 to 6
- taps_grad_sum: float32 [3, 4096], P(None, 'tp'), may hold values from -6 to 6
- bias_grad_sum: float32 [4096], P('tp'), may hold values from -6 to 6
Outputs:
- hidden_later: bfloat16 [6144, 4096], P('fs', 'tp')
- input_grad: bfloat16 [6144, 2048], P('fs')
- gate_grad_out: float32 [2048, 4096], P('fs', 'tp')
- up_grad_out: float32 [2048, 4096], P('fs', 'tp')
- taps_grad_out: float32 [3, 4096], P(None, 'tp')
- bias_grad_out: float32 [4096], P('tp')
All inputs are finite; a program needn't handle non-finite values.
Results may differ from a plain program's by a relative error of at most 0.019.
Values may be sent and summed in bfloat16 or wider, within the bound.
No kernel may reach another device: no remote copies, remote signals or barrier semaphores. Data moves between devices by JAX's collectives and lax.ppermute only.
A program may use at most 128 MiB of HBM per device.

v0:
```python
import jax
import jax.numpy as jnp
from jax import lax
from jax.sharding import PartitionSpec as P


def shift_down(values, distance):
    total_len = values.shape[1]
    return jnp.pad(values, ((0, 0), (distance, 0), (0, 0)))[:, :total_len]


def shift_up(values, distance):
    return jnp.pad(values, ((0, 0), (0, distance), (0, 0)))[:, distance:]


def causal_mix(pre_values, conv_taps, conv_bias):
    return (
        conv_taps[0] * shift_down(pre_values, 2)
        + conv_taps[1] * shift_down(pre_values, 1)
        + conv_taps[2] * pre_values
        + conv_bias
    )


def mix_adjoint(mixed_grad, conv_taps):
    return (
        conv_taps[2] * mixed_grad
        + conv_taps[1] * shift_up(mixed_grad, 1)
        + conv_taps[0] * shift_up(mixed_grad, 2)
    )


def contract_last(left, right):
    return lax.dot_general(
        left, right, (((1,), (1,)), ((), ())), preferred_element_type=jnp.float32
    )


def contract_first(left, right):
    return lax.dot_general(
        left, right, (((0,), (0,)), ((), ())), preferred_element_type=jnp.float32
    )


def on_device(
    rows_later,
    rows_earlier,
    out_cotangent,
    gate_proj,
    up_proj,
    conv_taps,
    conv_bias,
    gate_grad_sum,
    up_grad_sum,
    taps_grad_sum,
    bias_grad_sum,
):
    seq_len = rows_later.shape[0]
    shard_width = out_cotangent.shape[1]
    stacked_rows = jnp.concatenate([rows_later, rows_earlier], axis=0)
    paired = jnp.stack([gate_proj, up_proj], axis=0)
    pieces = lax.all_gather(paired, "fs", axis=1, tiled=True)
    gate_acc = jnp.dot(stacked_rows, pieces[0], preferred_element_type=jnp.float32)
    up_acc = jnp.dot(stacked_rows, pieces[1], preferred_element_type=jnp.float32)
    gate_pre = gate_acc.astype(jnp.bfloat16)
    up_value = up_acc.astype(jnp.bfloat16)
    gate_pre, up_value = lax.optimization_barrier((gate_pre, up_value))
    gate_float = gate_pre.astype(jnp.float32).reshape(2, seq_len, shard_width)
    up_float = up_value.astype(jnp.float32).reshape(2, seq_len, shard_width)
    mixed = causal_mix(gate_float, conv_taps, conv_bias)
    sig_all = jax.nn.sigmoid(mixed)
    activated = mixed * sig_all
    hidden = (activated * up_float).astype(jnp.bfloat16)
    hidden_later = hidden[0]
    grad_scale = lax.rsqrt(jnp.asarray(seq_len * lax.axis_size("fs"), jnp.float32))

    def make_term(grad_rows):
        return contract_first(rows_earlier, grad_rows)

    cotangent = out_cotangent.astype(jnp.float32)[None]
    mixed_back = mixed[1:]
    sig_back = sig_all[1:]
    up_grad = (cotangent * activated[1:]).astype(jnp.bfloat16)[0]
    up_summed = lax.psum_scatter(
        make_term(up_grad).astype(jnp.bfloat16), "fs", scatter_dimension=0, tiled=True
    ).astype(jnp.float32)
    mixed_grad = cotangent * up_float[1:] * sig_back * (1.0 + mixed_back * (1.0 - sig_back))
    gate_grad = mix_adjoint(mixed_grad, conv_taps).astype(jnp.bfloat16)[0]
    gate_summed = lax.psum_scatter(
        make_term(gate_grad).astype(jnp.bfloat16), "fs", scatter_dimension=0, tiled=True
    ).astype(jnp.float32)
    pieces = lax.all_gather(paired, "fs", axis=1, tiled=True)
    partial_rows = contract_last(gate_grad, pieces[0]) + contract_last(up_grad, pieces[1])
    input_grad = lax.psum(partial_rows.astype(jnp.bfloat16), "tp")
    gate_grad_out = gate_grad_sum + grad_scale * gate_summed
    up_grad_out = up_grad_sum + grad_scale * up_summed
    gate_back = gate_float[1:]
    tap_local = jnp.stack(
        [
            jnp.sum(mixed_grad * shift_down(gate_back, 2 - tap_index), axis=(0, 1))
            for tap_index in range(conv_taps.shape[0])
        ]
    )
    bias_local = jnp.sum(mixed_grad, axis=(0, 1))
    tap_total, bias_total = lax.psum((tap_local, bias_local), "fs")
    taps_grad_out = taps_grad_sum + grad_scale * tap_total
    bias_grad_out = bias_grad_sum + grad_scale * bias_total
    return (hidden_later, input_grad, gate_grad_out, up_grad_out, taps_grad_out, bias_grad_out)


def solution(mesh):
    placed = (
        P("fs", None),
        P("fs", None),
        P("fs", "tp"),
        P("fs", "tp"),
        P("fs", "tp"),
        P(None, "tp"),
        P("tp"),
        P("fs", "tp"),
        P("fs", "tp"),
        P(None, "tp"),
        P("tp"),
    )
    return jax.shard_map(
        on_device,
        mesh=mesh,
        in_specs=placed,
        out_specs=(
            P("fs", "tp"),
            P("fs", None),
            P("fs", "tp"),
            P("fs", "tp"),
            P(None, "tp"),
            P("tp"),
        ),
        check_vma=False,
    )
```

profile of v0, /device:TPU:0, one launch (start us, length us, event | category | flops | bytes accessed | tf_op | source)
XLA Modules:
  0.0 333.8 jit_solution(14247439538161545756)
XLA Ops:
  7.2 2.4 pad_maximum_fusion
  9.7 0.9 fusion.32
  10.7 2.0 constant_dynamic-update-slice_fusion.1
  12.6 2.1 constant_dynamic-update-slice_fusion
  14.8 80.2 %all-gather.2.cloned.1.call-done = bf16[2,2048,1024]{2,1,0:T(8,128)(2,1)} async-done(((bf16[2,256,1024]{2,1,0:T(8,128)(2,1)}), bf16[2,2048,1024]{2,1,0:T(8,128)(2,1)}) %all-gather.2.cloned.1.call-update) | async-done | bytes 8388624 | tf_op jit(solution)/shard_map/all_gather | solution.py:62
  95.0 10.1 %convolution_convert_fusion = bf16[1536,1024]{1,0:T(8,128)(2,1)S(1)} fusion(bf16[1536,2048]{1,0:T(8,128)(2,1)} %constant_dynamic-update-slice_fusion, bf16[2,2048,1024]{2,1,0:T(8,128)(2,1)} %all-gather.2.cloned.1.call-done), kind=kOutput, calls=%fused_computation.15 | convolution fusion | flops 6444023808 | bytes 13631488 | tf_op jit(solution)/shard_map/dot_general | solution.py:64
  105.1 8.8 %convolution_convert_fusion.1 = bf16[1536,1024]{1,0:T(8,128)(2,1)S(1)} fusion(bf16[1536,2048]{1,0:T(8,128)(2,1)} %constant_dynamic-update-slice_fusion, bf16[2,2048,1024]{2,1,0:T(8,128)(2,1)S(1)} %copy-done.15), kind=kOutput, calls=%fused_computation.16 | convolution fusion | flops 6444023808 | bytes 13631488 | tf_op jit(solution)/shard_map/dot_general | solution.py:63
  113.9 0.7 convert_element_type.59
  114.7 1.9 slice_bitcast_fusion.6
  116.5 0.7 convert_element_type.60
  117.3 3.2 add_divide_fusion
  121.1 6.3 %fusion.13 = (f32[1024]{0:T(1024)S(1)}, f32[1024]{0:T(1024)S(1)}, f32[1024]{0:T(1024)S(1)}, f32[1024]{0:T(1024)S(1)}, f32[1,768,1024]{2,1,0:T(8,128)S(1)}) fusion(f32[1,768,1024]{2,1,0:T(8,128)} %slice_bitcast_fusion.6, f32[1536,1024]{1,0:T(8,128)S(1)} %convert_element_type.59, f32[2,768,1024]{2,1,0:T(8,128)S(1)} %get-tuple-element.24, ...), kind=kLoop, calls=%fused_computation.29 | loop fusion | flops 11005952 | bytes 20463616 | tf_op jit(solution)/shard_map/reduce_sum | solution.py:100
  127.4 1.0 fusion.10
  128.4 1.1 copy-done.9
  129.5 5.1 %convert_bitcast_fusion.1 = bf16[2048,1024]{0,1:T(8,128)(2,1)} fusion(bf16[768,2048]{1,0:T(8,128)(2,1)S(1)} %copy-done.6, bf16[1,768,1024]{2,1,0:T(8,128)(2,1)S(1)} %fusion.10), kind=kOutput, calls=%fused_computation.12 | convolution fusion | flops 3223322624 | bytes 8912896 | tf_op jit(solution)/shard_map/dot_general | solution.py:40
  134.9 4.5 %fusion.29 = f32[2,768,1024]{2,1,0:T(8,128)S(1)} fusion(f32[2,768,1024]{2,1,0:T(8,128)} %copy-done), kind=kLoop, calls=%fused_computation.55 | loop fusion | flops 6291456 | bytes 12582912 | tf_op jit(solution)/shard_map/mul | solution.py:72
  139.4 2.6 copy-done.2
  142.0 5.1 %convert_bitcast_fusion = bf16[2048,1024]{0,1:T(8,128)(2,1)} fusion(bf16[768,2048]{1,0:T(8,128)(2,1)S(1)} %copy-done.6, f32[2,768,1024]{2,1,0:T(8,128)S(1)} %fusion.29, bf16[768,1024]{1,0:T(8,128)(2,1)S(1)} %copy-done.7), kind=kOutput, calls=%fused_computation.11 | convolution fusion | flops 3225681920 | bytes 12058624 | tf_op jit(solution)/shard_map/dot_general | solution.py:40
  147.2 1.3 copy-done.10
  148.6 5.5 %fusion.5 = f32[768,2048]{1,0:T(8,128)S(1)} fusion(bf16[2,2048,1024]{2,1,0:T(8,128)(2,1)} %all-gather.2.cloned.1.call-done, bf16[1,768,1024]{2,1,0:T(8,128)(2,1)S(1)} %copy-done.10), kind=kOutput, calls=%fused_computation.17 | convolution fusion | flops 3221225472 | bytes 12058624 | tf_op jit(solution)/shard_map/dot_general | solution.py:34
  154.1 7.3 %add_convert_fusion = bf16[768,2048]{1,0:T(8,128)(2,1)} fusion(f32[768,2048]{1,0:T(8,128)S(1)} %fusion.5, bf16[2,2048,1024]{2,1,0:T(8,128)(2,1)} %all-gather.2.cloned.1.call-done, f32[2,768,1024]{2,1,0:T(8,128)S(1)} %copy-done.3, bf16[768,1024]{1,0:T(8,128)(2,1)S(1)} %copy-done.8), kind=kOutput, calls=%fused_computation.7 | convolution fusion | flops 3226730496 | bytes 18350080 | tf_op jit(solution)/shard_map/dot_general | solution.py:34
  161.8 1.6 copy.18
  163.4 27.1 %all-reduce.6 = (f32[3,1024]{1,0:T(4,128)S(1)}, f32[1024]{0:T(1024)S(1)}) all-reduce(f32[3,1024]{1,0:T(4,128)S(1)} %pad_maximum_fusion.1, f32[1024]{0:T(1024)S(1)} %get-tuple-element.18), channel_id=1, replica_groups=mesh['fs'=8,'tp'=4] {'fs'}, use_global_device_ids=true, to_apply=%region_6.7 | all-reduce | flops 4096 | bytes 32768 | tf_op jit(solution)/shard_map/psum | solution.py:105
  191.1 0.6 multiply_add_fusion.2
  191.7 4.5 %fusion.23 = bf16[768,1024]{1,0:T(8,128)(2,1)} fusion(f32[2,768,1024]{2,1,0:T(8,128)} %bitcast.61, f32[2,768,1024]{2,1,0:T(8,128)} %copy-done.2), kind=kLoop, calls=%fused_computation.43 | loop fusion | flops 1572864 | bytes 7864320 | tf_op jit(solution)/shard_map/squeeze | solution.py:74
  196.2 1.2 multiply_add_fusion.1
  197.4 1.3 copy.19
  198.7 35.6 %reduce-scatter.5.cloned.1.call-done = bf16[256,1024]{0,1:T(8,128)(2,1)} async-done(((bf16[2048,1024]{0,1:T(8,128)(2,1)}), bf16[256,1024]{0,1:T(8,128)(2,1)}) %reduce-scatter.5.cloned.1.call-update) | async-done | bytes 524304 | tf_op jit(solution)/shard_map/reduce_scatter | solution.py:84
  234.3 1.2 multiply_add_fusion
  235.5 1.3 copy.20
  236.8 86.5 %all-reduce.9.cloned.1.call-done = bf16[768,2048]{1,0:T(8,128)(2,1)} async-done(((bf16[768,2048]{1,0:T(8,128)(2,1)}), bf16[768,2048]{1,0:T(8,128)(2,1)}) %all-reduce.9.cloned.1.call-update) | async-done | bytes 3145744 | tf_op jit(solution)/shard_map/psum | solution.py:94
  323.3 4.0 %copy.23 = bf16[768,2048]{1,0:T(8,128)(2,1)} copy(bf16[768,2048]{1,0:T(8,128)(2,1)} %all-reduce.9.cloned.1.call-done) | data formatting | bytes 6291456
  (41 shorter events, 2.0 us)
Async XLA Ops:
  7.2 3.5 %copy-start.4 = (bf16[768,2048]{1,0:T(8,128)(2,1)S(1)}, bf16[768,2048]{1,0:T(8,128)(2,1)}, u32[]{:S(2)}) copy-start(bf16[768,2048]{1,0:T(8,128)(2,1)} %param.11) | copy-start | bytes 9437188
  7.2 87.8 %all-gather.2.cloned.1.call-start = ((), (), s32[]{:S(2)}) async-start(), calls=%async_computation.2 | async-start | bytes 9437184 | tf_op jit(solution)/shard_map/all_gather | solution.py:62
  9.7 186.6 %reduce-scatter.3.cloned.1.call-start = ((), (), s32[]{:S(2)}) async-start(), calls=%async_computation.4 | async-start | bytes 4718592 | tf_op jit(solution)/shard_map/reduce_scatter | solution.py:89
  9.7 2.9 copy-start.5
  95.0 10.1 %copy-start.15 = (bf16[2,2048,1024]{2,1,0:T(8,128)(2,1)S(1)}, bf16[2,2048,1024]{2,1,0:T(8,128)(2,1)}, u32[]{:S(2)}) copy-start(bf16[2,2048,1024]{2,1,0:T(8,128)(2,1)} %all-gather.2.cloned.1.call-done) | copy-start | bytes 25165828
  116.5 0.7 copy-start.14
  117.3 3.8 %copy-start.1 = (f32[1536,1024]{1,0:T(8,128)}, f32[1536,1024]{1,0:T(8,128)S(1)}, u32[]{:S(2)}) copy-start(f32[1536,1024]{1,0:T(8,128)S(1)} %convert_element_type.60) | copy-start | bytes 18874372
  120.5 6.9 %copy-start = (f32[2,768,1024]{2,1,0:T(8,128)}, f32[2,768,1024]{2,1,0:T(8,128)S(1)}, u32[]{:S(2)}) copy-start(f32[2,768,1024]{2,1,0:T(8,128)S(1)} %get-tuple-element.24) | copy-start | bytes 18874372
  127.4 2.2 copy-start.6
  128.4 1.1 copy-start.9
  134.6 99.7 %reduce-scatter.5.cloned.1.call-start = ((), (), s32[]{:S(2)}) async-start(), calls=%async_computation.5 | async-start | bytes 4718592 | tf_op jit(solution)/shard_map/reduce_scatter | solution.py:84
  134.9 7.1 %copy-start.7 = (bf16[768,1024]{1,0:T(8,128)(2,1)S(1)}, bf16[768,1024]{1,0:T(8,128)(2,1)}, u32[]{:S(2)}) copy-start(bf16[768,1024]{1,0:T(8,128)(2,1)} %param.13) | copy-start | bytes 4718596
  139.4 2.6 copy-start.2
  147.1 1.4 copy-start.10
  147.2 6.9 %copy-start.8 = (bf16[768,1024]{1,0:T(8,128)(2,1)S(1)}, bf16[768,1024]{1,0:T(8,128)(2,1)}, u32[]{:S(2)}) copy-start(bf16[768,1024]{1,0:T(8,128)(2,1)} %param.13) | copy-start | bytes 4718596
  147.2 176.1 %all-reduce.9.cloned.1.call-start = ((), (), s32[]{:S(2)}) async-start(), calls=%async_computation.3 | async-start | bytes 6291456 | tf_op jit(solution)/shard_map/psum | solution.py:94
  148.6 5.5 %copy-start.3 = (f32[2,768,1024]{2,1,0:T(8,128)S(1)}, f32[2,768,1024]{2,1,0:T(8,128)}, u32[]{:S(2)}) copy-start(f32[2,768,1024]{2,1,0:T(8,128)} %copy-done.2) | copy-start | bytes 18874372
  154.1 7.4 %copy-start.11 = (f32[256,1024]{1,0:T(8,128)S(1)}, f32[256,1024]{1,0:T(8,128)}, u32[]{:S(2)}) copy-start(f32[256,1024]{1,0:T(8,128)} %param.18) | copy-start | bytes 3145732
  161.4 29.1 %copy-start.13 = (f32[1024]{0:T(1024)S(1)}, f32[1024]{0:T(1024)}, u32[]{:S(2)}) copy-start(f32[1024]{0:T(1024)} %param.21) | copy-start | bytes 12292
  161.4 29.7 %copy-start.12 = (f32[3,1024]{1,0:T(4,128)S(1)}, f32[3,1024]{1,0:T(4,128)}, u32[]{:S(2)}) copy-start(f32[3,1024]{1,0:T(4,128)} %param.20) | copy-start | bytes 36868
Sparse Core Ops, SparseCore 0:
  10.2 84.7 all-gather.1
  134.8 48.8 reduce-scatter.2
  185.9 48.3 reduce-scatter.4
  237.9 85.4 all-reduce.8
where the time goes:
time: 334 us
  waiting for transfers between devices  202 us (60%)
  matrix products  42 us (13%)
  blocking collectives  27.1 us (8%)
  other arithmetic  26.9 us (8%)
  local copies, waits for them, and re-layouts  21.1 us (6%)
  between operations  14 us (4%)
    psum x1, waiting for transfers between devices, on_device(): input_grad = lax.psum(partial_rows.astype(jnp.bfloat16), 'tp')  86.5 us
    all_gather x1, waiting for transfers between devices, on_device(): pieces = lax.all_gather(paired, 'fs', axis=1, tiled=True)  80.2 us
    reduce_scatter x1, waiting for transfers between devices, on_device(): lax.psum_scatter(make_term(up_grad).astype(jnp.bfloat16), 'fs', scatter_d...  35.6 us
    psum x1, blocking collectives, on_device(): tap_total, bias_total = lax.psum((tap_local, bias_local), 'fs')  27.1 us
    unnamed x38, local copies, waits for them, and re-layouts  16.1 us
    dot_general x2, matrix products, contract_last(): lax.dot_general(left, right, (((1,), (1,)), ((), ())), preferred_element_...  12.8 us
    dot_general x2, matrix products, contract_first(): lax.dot_general(left, right, (((0,), (0,)), ((), ())), preferred_element_...  10.2 us
    dot_general x1, matrix products, on_device(): jnp.dot(stacked_rows, pieces[1], preferred_element_type=jnp.float32)  10.1 us
  transfers between devices with their start and end apart: 4, of which 3 were waited for; matrix products, arithmetic and copies ran while one was open for 12% of the time, Pallas kernels for 0%

commit v1 on v0

v1 whole, which is shorter than its diff:
```python
import jax
import jax.numpy as jnp
import numpy as np
from jax import lax
from jax.experimental import pallas as pl
from jax.experimental.pallas import tpu as pltpu
from jax.sharding import PartitionSpec as P

LANES = 128
CHUNKS = 2


def contract_last(left, right):
    return lax.dot_general(
        left, right, (((1,), (1,)), ((), ())), preferred_element_type=jnp.float32
    )


def contract_first(left, right):
    return lax.dot_general(
        left, right, (((0,), (0,)), ((), ())), preferred_element_type=jnp.float32
    )


def exchange(values, axis_name, distance):
    pairs = [(i, i ^ distance) for i in range(lax.axis_size(axis_name))]
    return lax.ppermute(values, axis_name, pairs)


def doubling_sum(values, axis_name):
    distance = 1
    while distance < lax.axis_size(axis_name):
        values = values + exchange(values, axis_name, distance)
        distance *= 2
    return values


def step_bit(axis_name, distance):
    return (lax.axis_index(axis_name) // distance) % 2


def halving_scatter(values, axis_name, distances):
    kept = values
    for distance in distances:
        half = kept.shape[0] // 2
        bit = step_bit(axis_name, distance)
        sent = lax.dynamic_slice_in_dim(kept, (1 - bit) * half, half, 0).astype(jnp.bfloat16)
        own = lax.dynamic_slice_in_dim(kept, bit * half, half, 0).astype(jnp.float32)
        kept = own + exchange(sent, axis_name, distance).astype(jnp.float32)
    return kept.astype(jnp.bfloat16)


def doubling_gather(values, axis_name, distances):
    for distance in reversed(distances):
        other = exchange(values, axis_name, distance)
        low = step_bit(axis_name, distance) == 0
        values = jnp.concatenate(
            [jnp.where(low, values, other), jnp.where(low, other, values)], axis=0
        )
    return values


def pair_kernel(gate_ref, up_ref, paired_ref):
    paired_ref[:, :LANES] = gate_ref[...]
    paired_ref[:, LANES:] = up_ref[...]


def pair_blocks(gate, up, first, blocks):
    rows = gate.shape[0]
    at = lambda j: (0, first + j)
    return pl.pallas_call(
        pair_kernel,
        grid=(blocks,),
        in_specs=[pl.BlockSpec((rows, LANES), at)] * 2,
        out_specs=pl.BlockSpec((rows, 2 * LANES), lambda j: (0, j)),
        out_shape=jax.ShapeDtypeStruct((rows, 2 * LANES * blocks), gate.dtype),
        name="pair_blocks",
    )(gate, up)


def rolled(values, distance):
    total = values.shape[0]
    row = lax.broadcasted_iota(jnp.int32, values.shape, 0)
    moved = pltpu.roll(values, distance % total, 0)
    inside = row >= distance if distance > 0 else row < total + distance
    return jnp.where(inside, moved, 0.0)


def mix_block(pre_ref, taps_ref, bias_ref):
    gate = pre_ref[:, :LANES].astype(jnp.float32)
    up = pre_ref[:, LANES:].astype(jnp.float32)
    down_two, down_one = rolled(gate, 2), rolled(gate, 1)
    taps = [taps_ref[k : k + 1, :] for k in range(3)]
    mixed = taps[0] * down_two + taps[1] * down_one + taps[2] * gate + bias_ref[...]
    return gate, up, down_two, down_one, taps, mixed, jax.nn.sigmoid(mixed)


def backward_kernel(pre_ref, cotangent_ref, taps_ref, bias_ref, grads_ref, terms_ref):
    gate, up, down_two, down_one, taps, mixed, sig = mix_block(pre_ref, taps_ref, bias_ref)
    cotangent = cotangent_ref[...].astype(jnp.float32)
    grads_ref[:, LANES:] = (cotangent * (mixed * sig)).astype(jnp.bfloat16)
    mixed_grad = cotangent * up * sig * (1.0 + mixed * (1.0 - sig))
    gate_grad = (
        taps[2] * mixed_grad + taps[1] * rolled(mixed_grad, -1) + taps[0] * rolled(mixed_grad, -2)
    )
    grads_ref[:, :LANES] = gate_grad.astype(jnp.bfloat16)
    for k, shifted in enumerate((down_two, down_one, gate)):
        terms_ref[k : k + 1, :] = jnp.sum(mixed_grad * shifted, axis=0, keepdims=True)
    terms_ref[3:4, :] = jnp.sum(mixed_grad, axis=0, keepdims=True)


def backward_mix(pre, cotangent, taps, bias, first):
    rows, pair_width = pre.shape
    blocks = pair_width // (2 * LANES)
    at = lambda j: (0, first + j)
    return pl.pallas_call(
        backward_kernel,
        grid=(blocks,),
        in_specs=[
            pl.BlockSpec((rows, 2 * LANES), lambda j: (0, j)),
            pl.BlockSpec((rows, LANES), at),
            pl.BlockSpec((taps.shape[0], LANES), at),
            pl.BlockSpec((1, LANES), at),
        ],
        out_specs=[
            pl.BlockSpec((rows, 2 * LANES), lambda j: (0, j)),
            pl.BlockSpec((4, LANES), lambda j: (0, j)),
        ],
        out_shape=[
            jax.ShapeDtypeStruct(pre.shape, jnp.bfloat16),
            jax.ShapeDtypeStruct((4, pair_width // 2), jnp.float32),
        ],
        name="backward_mix",
    )(pre, cotangent, taps, bias)


def forward_kernel(pre_ref, taps_ref, bias_ref, *refs):
    _, up, _, _, _, mixed, sig = mix_block(pre_ref, taps_ref, bias_ref)
    refs[-1][...] = (mixed * sig * up).astype(jnp.bfloat16)


def forward_mix(pre, taps, bias, first, before):
    rows, pair_width = pre.shape
    at = lambda j: (0, first + j)
    prior = [] if before is None else [before]
    return pl.pallas_call(
        forward_kernel,
        grid=(pair_width // (2 * LANES),),
        in_specs=[
            pl.BlockSpec((rows, 2 * LANES), lambda j: (0, j)),
            pl.BlockSpec((taps.shape[0], LANES), at),
            pl.BlockSpec((1, LANES), at),
        ]
        + [pl.BlockSpec(memory_space=pl.ANY) for _ in prior],
        out_specs=pl.BlockSpec((rows, LANES), at),
        out_shape=jax.ShapeDtypeStruct((rows, taps.shape[1]), jnp.bfloat16),
        input_output_aliases={3: 0} if prior else {},
        name="forward_mix",
    )(pre, taps, bias, *prior)


def add_kernel(scale, summed_ref, gate_ref, up_ref, *refs):
    summed = summed_ref[...].astype(jnp.float32)
    refs[-2][...] = gate_ref[...] + scale * summed[:, :LANES]
    refs[-1][...] = up_ref[...] + scale * summed[:, LANES:]


def add_terms(summed, gate_sum, up_sum, scale, first, before):
    rows, pair_width = summed.shape
    at = lambda j: (0, first + j)
    shape = jax.ShapeDtypeStruct(gate_sum.shape, jnp.float32)
    return pl.pallas_call(
        lambda *refs: add_kernel(scale, *refs),
        grid=(pair_width // (2 * LANES),),
        in_specs=[
            pl.BlockSpec((rows, 2 * LANES), lambda j: (0, j)),
            pl.BlockSpec((rows, LANES), at),
            pl.BlockSpec((rows, LANES), at),
        ]
        + [pl.BlockSpec(memory_space=pl.ANY) for _ in before],
        out_specs=[pl.BlockSpec((rows, LANES), at)] * 2,
        out_shape=[shape, shape],
        input_output_aliases={3: 0, 4: 1} if before else {},
        name="add_terms",
    )(summed, gate_sum, up_sum, *before)


def axis_sum(streams, axis_name, between):
    distances = []
    distance = 1
    while distance < lax.axis_size(axis_name):
        distances.append(distance)
        distance *= 2
    turn = len(distances) // 2
    orders = [distances, distances[turn:] + distances[:turn]]
    summed = [halving_scatter(s, axis_name, o) for s, o in zip(streams, orders)]
    summed, between = lax.optimization_barrier((summed, between))
    return [doubling_gather(s, axis_name, o) for s, o in zip(summed, orders)], between


def on_device(
    rows_later,
    rows_earlier,
    out_cotangent,
    gate_proj,
    up_proj,
    conv_taps,
    conv_bias,
    gate_grad_sum,
    up_grad_sum,
    taps_grad_sum,
    bias_grad_sum,
):
    seq_len = rows_later.shape[0]
    shard_rows, shard_width = gate_proj.shape
    fs_size = lax.axis_size("fs")
    per_chunk = shard_width // LANES // CHUNKS
    scale = np.float32(1.0 / np.sqrt(seq_len * fs_size))
    half = seq_len // 2
    bias_row = conv_bias[None]

    weights = []
    sent = None
    for c in range(CHUNKS):
        paired = pair_blocks(gate_proj, up_proj, c * per_chunk, per_chunk)
        if sent is not None:
            paired, sent = lax.optimization_barrier((paired, sent))
        sent = paired
        weights.append(lax.all_gather(paired, "fs", axis=0, tiled=True))

    def project(rows, weight):
        return jnp.dot(rows, weight, preferred_element_type=jnp.float32).astype(jnp.bfloat16)

    def scatter(term):
        return lax.psum_scatter(term, "fs", scatter_dimension=0, tiled=True)

    def later_mix(c, weight, before):
        pre = project(rows_later, weight)
        return forward_mix(pre, conv_taps, bias_row, c * per_chunk, before)

    partial = None
    hidden_later = None
    terms = []
    summed = []
    for c in range(CHUNKS):
        weight = weights[c]
        if partial is not None:
            weight, partial, hidden_later = lax.optimization_barrier(
                (weight, partial, hidden_later)
            )
        pre = project(rows_earlier, weight)
        grads, taps_part = backward_mix(pre, out_cotangent, conv_taps, bias_row, c * per_chunk)
        terms.append(taps_part)
        if c < CHUNKS - 1:
            summed.append(scatter(contract_first(rows_earlier, grads).astype(jnp.bfloat16)))
            part = contract_last(grads, weight)
            partial = part if partial is None else partial + part
            hidden_later = later_mix(c, weight, hidden_later)
        else:
            streams = []
            for at in (slice(0, half), slice(half, None)):
                stream = contract_last(grads[at], weight)
                stream = stream if partial is None else partial[at] + stream
                streams.append(stream.astype(jnp.bfloat16))
            grads, streams = lax.optimization_barrier((grads, streams))
            summed.append(scatter(contract_first(rows_earlier, grads).astype(jnp.bfloat16)))
    sums = ()
    for c in range(CHUNKS - 1):
        sums = add_terms(summed[c], gate_grad_sum, up_grad_sum, scale, c * per_chunk, sums)
    streams, sums = axis_sum(streams, "tp", sums)
    input_grad = jnp.concatenate(streams, axis=0)
    gate_grad_out, up_grad_out = add_terms(
        summed[-1], gate_grad_sum, up_grad_sum, scale, (CHUNKS - 1) * per_chunk, sums
    )
    hidden_later = later_mix(CHUNKS - 1, weights[-1], hidden_later)
    tap_total = doubling_sum(jnp.concatenate(terms, axis=1), "fs")
    taps_grad_out = taps_grad_sum + scale * tap_total[:-1]
    bias_grad_out = bias_grad_sum + scale * tap_total[-1]
    return (hidden_later, input_grad, gate_grad_out, up_grad_out, taps_grad_out, bias_grad_out)


def solution(mesh):
    placed = (
        P("fs", None),
        P("fs", None),
        P("fs", "tp"),
        P("fs", "tp"),
        P("fs", "tp"),
        P(None, "tp"),
        P("tp"),
        P("fs", "tp"),
        P("fs", "tp"),
        P(None, "tp"),
        P("tp"),
    )
    return jax.shard_map(
        on_device,
        mesh=mesh,
        in_specs=placed,
        out_specs=(
            P("fs", "tp"),
            P("fs", None),
            P("fs", "tp"),
            P("fs", "tp"),
            P(None, "tp"),
            P("tp"),
        ),
        check_vma=False,
    )
```

time: 334 us -> 231 us (0.69)
  waiting for transfers between devices: 202 us -> 91.7 us
  Pallas kernels: 0 us -> 31.2 us
  blocking collectives: 27.1 us -> 0 us
  matrix products: 42 us -> 60.8 us
  local copies, waits for them, and re-layouts: 21.1 us -> 5.86 us
  other arithmetic: 26.9 us -> 14.9 us
  starting transfers between devices: 0.34 us -> 11.4 us
    psum x1 -> x0, waiting for transfers between devices: 86.5 us -> none  [on_device(): input_grad = lax.psum(partial_rows.astype(jnp.bfloat16), 'tp')]
    ppermute x0 -> x11, waiting for transfers between devices: none -> 33.2 us  [exchange(): return lax.ppermute(values, axis_name, pairs)]
    reduce_scatter x2, waiting for transfers between devices: 35.6 us -> 2.63 us  [scatter(): return lax.psum_scatter(term, 'fs', scatter_dimension=0, tiled=True)]
    pallas_call x0 -> x8, Pallas kernels: none -> 31.2 us  [the longest x2 9.94 us: backward_mix(): pl.pallas_call(backward_kernel, grid=(blocks,), in_specs=[pl.BlockSpec((r...]
    psum x1 -> x0, blocking collectives: 27.1 us -> none  [on_device(): tap_total, bias_total = lax.psum((tap_local, bias_local), 'fs')]
    all_gather x1 -> x2, waiting for transfers between devices: 80.2 us -> 55.7 us  [on_device(): weights.append(lax.all_gather(paired, 'fs', axis=0, tiled=True))]
    unnamed x38 -> x29, local copies, waits for them, and re-layouts: 16.1 us -> 1.54 us
    ppermute x0 -> x11, starting transfers between devices: none -> 11.3 us  [exchange(): return lax.ppermute(values, axis_name, pairs)]
  transfers between devices with their start and end apart: 4 -> 15, of which waited for: 3 -> 12; matrix products, arithmetic and copies ran while one was open for 12% -> 33% of each run, Pallas kernels for 0% -> 12%
where the time goes in v1:
time: 231 us; the launch traced here: 230 us
  waiting for transfers between devices  91.7 us (40%)
  matrix products  60.8 us (26%)
  Pallas kernels  31.2 us (14%)
  other arithmetic  14.9 us (6%)
  between operations  14 us (6%)
  starting transfers between devices  11.4 us (5%)
  local copies, waits for them, and re-layouts  5.86 us (3%)
    all_gather x2, waiting for transfers between devices, on_device(): weights.append(lax.all_gather(paired, 'fs', axis=0, tiled=True))  55.7 us
    ppermute x11, waiting for transfers between devices, exchange(): return lax.ppermute(values, axis_name, pairs)  33.2 us
    dot_general x4, matrix products, project(): jnp.dot(rows, weight, preferred_element_type=jnp.float32)  28.9 us
    dot_general x3, matrix products, contract_last(): lax.dot_general(left, right, (((1,), (1,)), ((), ())), preferred_element_...  20.4 us
    dot_general x2, matrix products, contract_first(): lax.dot_general(left, right, (((0,), (0,)), ((), ())), preferred_element_...  11.5 us
    ppermute x11, starting transfers between devices, exchange(): return lax.ppermute(values, axis_name, pairs)  11.3 us
    pallas_call x2, Pallas kernels, backward_mix(): pl.pallas_call(backward_kernel, grid=(blocks,), in_specs=[pl.BlockSpec((r...  9.94 us
    pallas_call x2, Pallas kernels, forward_mix(): pl.pallas_call(forward_kernel, grid=(pair_width // (2 * LANES),), in_spec...  7.71 us
  transfers between devices with their start and end apart: 15, of which 12 were waited for; matrix products, arithmetic and copies ran while one was open for 33% of the time, Pallas kernels for 12%

profile of v1, /device:TPU:0, one launch (start us, length us, event | category | flops | bytes accessed | tf_op | source)
XLA Modules:
  0.0 229.9 jit_solution(1374125546452543941)
XLA Ops:
  7.2 3.3 %pair_blocks.3 = bf16[256,1024]{1,0:T(8,128)(2,1)} custom-call(bf16[256,1024]{1,0:T(8,128)(2,1)} %gate_ref.3, bf16[256,1024]{1,0:T(8,128)(2,1)} %up_ref.3), custom_call_target="tpu_custom_call" | custom-call | tf_op jit(solution)/shard_map/pair_blocks/pallas_call | solution.py:71
  10.6 3.1 %pair_blocks.2 = bf16[256,1024]{1,0:T(8,128)(2,1)} custom-call(bf16[256,1024]{1,0:T(8,128)(2,1)} %gate_ref.3, bf16[256,1024]{1,0:T(8,128)(2,1)} %up_ref.3), custom_call_target="tpu_custom_call" | custom-call | tf_op jit(solution)/shard_map/pair_blocks/pallas_call | solution.py:71
  13.8 46.5 %all-gather.5.cloned.1.call-done = bf16[2048,1024]{1,0:T(8,128)(2,1)} async-done(((bf16[256,1024]{1,0:T(8,128)(2,1)}), bf16[2048,1024]{1,0:T(8,128)(2,1)}) %all-gather.5.cloned.1.call-update) | async-done | bytes 4194320 | tf_op jit(solution)/shard_map/all_gather | solution.py:229
  60.3 6.7 %fusion.1.pre_ref = bf16[768,1024]{1,0:T(8,128)(2,1)} fusion(bf16[768,2048]{1,0:T(8,128)(2,1)S(1)} %copy-done, bf16[2048,1024]{1,0:T(8,128)(2,1)} %all-gather.5.cloned.1.call-done), kind=kOutput, calls=%fused_computation.12 | convolution fusion | flops 3222011904 | bytes 8912896 | tf_op jit(solution)/shard_map/dot_general | solution.py:232
  66.9 5.0 %backward_mix.2 = (bf16[768,1024]{1,0:T(8,128)(2,1)}, f32[4,512]{1,0:T(4,128)}) custom-call(bf16[768,1024]{1,0:T(8,128)(2,1)} %fusion.1.pre_ref, bf16[768,1024]{1,0:T(8,128)(2,1)} %cotangent_ref.3, f32[3,1024]{1,0:T(4,128)} %taps_ref.7, f32[1,1024]{1,0:T(1,128)} %bitcast.30), custom_call_target="tpu_custom_call" | custom-call | tf_op jit(solution)/shard_map/backward_mix/pallas_call | solution.py:116
  71.9 6.4 %convert_bitcast_fusion.1 = bf16[2048,1024]{1,0:T(8,128)(2,1)} fusion(bf16[768,1024]{1,0:T(8,128)(2,1)} %get-tuple-element.26, bf16[768,2048]{1,0:T(8,128)(2,1)S(1)} %copy-done), kind=kOutput, calls=%fused_computation.1 | convolution fusion | flops 3223322624 | bytes 8912896 | tf_op jit(solution)/shard_map/dot_general | solution.py:20
  78.4 7.8 %fusion.2.pre_ref = bf16[768,1024]{1,0:T(8,128)(2,1)} fusion(bf16[768,2048]{1,0:T(8,128)(2,1)} %param.11, bf16[2048,1024]{1,0:T(8,128)(2,1)} %all-gather.5.cloned.1.call-done), kind=kOutput, calls=%fused_computation.13 | convolution fusion | flops 3222011904 | bytes 8912896 | tf_op jit(solution)/shard_map/dot_general | solution.py:232
  86.2 3.9 %forward_mix.2.refs_0_ = bf16[768,1024]{1,0:T(8,128)(2,1)} custom-call(bf16[768,1024]{1,0:T(8,128)(2,1)} %fusion.2.pre_ref, f32[3,1024]{1,0:T(4,128)} %taps_ref.7, f32[1,1024]{1,0:T(1,128)} %bitcast.31), custom_call_target="tpu_custom_call" | custom-call | tf_op jit(solution)/shard_map/forward_mix/pallas_call | solution.py:146
  90.1 8.8 %fusion.7 = f32[768,2048]{1,0:T(8,128)} fusion(bf16[768,1024]{1,0:T(8,128)(2,1)} %get-tuple-element.26, bf16[2048,1024]{1,0:T(8,128)(2,1)} %all-gather.5.cloned.1.call-done), kind=kOutput, calls=%fused_computation.38 | convolution fusion | flops 3221225472 | bytes 12058624 | tf_op jit(solution)/shard_map/dot_general | solution.py:14
  98.9 9.3 %all-gather.3.cloned.1.call-done = bf16[2048,1024]{1,0:T(8,128)(2,1)} async-done(((bf16[256,1024]{1,0:T(8,128)(2,1)}), bf16[2048,1024]{1,0:T(8,128)(2,1)}) %all-gather.3.cloned.1.call-update) | async-done | bytes 4194320 | tf_op jit(solution)/shard_map/all_gather | solution.py:229
  108.2 6.7 %fusion.3.pre_ref = bf16[768,1024]{1,0:T(8,128)(2,1)} fusion(bf16[768,2048]{1,0:T(8,128)(2,1)S(1)} %copy-done, bf16[2048,1024]{1,0:T(8,128)(2,1)} %all-gather.3.cloned.1.call-done), kind=kOutput, calls=%fused_computation.14 | convolution fusion | flops 3222011904 | bytes 8912896 | tf_op jit(solution)/shard_map/dot_general | solution.py:232
  114.8 4.9 %backward_mix.3 = (bf16[768,1024]{1,0:T(8,128)(2,1)}, f32[4,512]{1,0:T(4,128)}) custom-call(bf16[768,1024]{1,0:T(8,128)(2,1)} %fusion.3.pre_ref, bf16[768,1024]{1,0:T(8,128)(2,1)} %cotangent_ref.3, f32[3,1024]{1,0:T(4,128)} %taps_ref.7, f32[1,1024]{1,0:T(1,128)} %bitcast.32), custom_call_target="tpu_custom_call" | custom-call | tf_op jit(solution)/shard_map/backward_mix/pallas_call | solution.py:116
  119.8 6.6 %add_convert_fusion = bf16[384,2048]{1,0:T(8,128)(2,1)} fusion(f32[768,2048]{1,0:T(8,128)} %fusion.7, bf16[2048,1024]{1,0:T(8,128)(2,1)} %all-gather.3.cloned.1.call-done, bf16[768,1024]{1,0:T(8,128)(2,1)} %get-tuple-element.37), kind=kOutput, calls=%fused_computation.3 | convolution fusion | flops 1612185600 | bytes 9699328 | tf_op jit(solution)/shard_map/dot_general | solution.py:14
  126.4 5.0 %add_convert_fusion.1 = bf16[384,2048]{1,0:T(8,128)(2,1)} fusion(f32[768,2048]{1,0:T(8,128)} %fusion.7, bf16[2048,1024]{1,0:T(8,128)(2,1)S(1)} %copy-done.12, bf16[768,1024]{1,0:T(8,128)(2,1)S(1)} %copy-done.13), kind=kOutput, calls=%fused_computation.4 | convolution fusion | flops 1612185600 | bytes 9699328 | tf_op jit(solution)/shard_map/dot_general | solution.py:14
  131.3 5.1 %convert_bitcast_fusion = bf16[2048,1024]{1,0:T(8,128)(2,1)} fusion(bf16[768,1024]{1,0:T(8,128)(2,1)S(1)} %copy-done.13, bf16[768,2048]{1,0:T(8,128)(2,1)S(1)} %copy-done), kind=kOutput, calls=%fused_computation | convolution fusion | flops 3223322624 | bytes 8912896 | tf_op jit(solution)/shard_map/dot_general | solution.py:20
  136.5 2.1 constant_dynamic-slice_fusion
  140.2 2.1 constant_dynamic-slice_fusion.1
  145.1 4.2 %collective-permute-done.9 = f32[4,1024]{1,0:T(4,128)S(1)} collective-permute-done((f32[4,1024]{1,0:T(4,128)S(1)}, f32[4,1024]{1,0:T(4,128)S(1)}, u32[]{:S(2)}, u32[]{:S(2)}) %collective-permute-start.9) | collective-permute-done | bytes 16416 | tf_op jit(solution)/shard_map/ppermute | solution.py:27
  150.3 8.3 %collective-permute-done.2 = bf16[192,2048]{1,0:T(8,128)(2,1)} collective-permute-done((bf16[192,2048]{1,0:T(8,128)(2,1)}, bf16[192,2048]{1,0:T(8,128)(2,1)}, u32[]{:S(2)}, u32[]{:S(2)}) %collective-permute-start.2) | collective-permute-done | bytes 786464 | tf_op jit(solution)/shard_map/ppermute | solution.py:27
  158.6 1.6 convert_add_fusion
  160.2 1.6 collective-permute-start.3
  164.7 5.9 %collective-permute-done.3 = bf16[96,2048]{1,0:T(8,128)(2,1)S(1)} collective-permute-done((bf16[96,2048]{1,0:T(8,128)(2,1)S(1)}, bf16[96,2048]{1,0:T(8,128)(2,1)S(1)}, u32[]{:S(2)}, u32[]{:S(2)}) %collective-permute-start.3) | collective-permute-done | bytes 393248 | tf_op jit(solution)/shard_map/ppermute | solution.py:27
  171.5 1.9 collective-permute-done.1
  173.5 3.7 %add_terms.2 = (f32[256,1024]{1,0:T(8,128)}, f32[256,1024]{1,0:T(8,128)}) custom-call(bf16[256,1024]{1,0:T(8,128)(2,1)} %reduce-scatter.3.cloned.1.call-done.refs_0_, f32[256,1024]{1,0:T(8,128)} %refs_1_.3, f32[256,1024]{1,0:T(8,128)} %refs_2_.3), custom_call_target="tpu_custom_call" | custom-call | tf_op jit(solution)/shard_map/add_terms/pallas_call | solution.py:172
  178.6 7.8 %fusion.pre_ref = bf16[768,1024]{1,0:T(8,128)(2,1)} fusion(bf16[768,2048]{1,0:T(8,128)(2,1)} %param.11, bf16[2048,1024]{1,0:T(8,128)(2,1)} %all-gather.3.cloned.1.call-done), kind=kOutput, calls=%fused_computation.11 | convolution fusion | flops 3222011904 | bytes 8912896 | tf_op jit(solution)/shard_map/dot_general | solution.py:232
  186.4 3.9 %forward_mix.3 = bf16[768,1024]{1,0:T(8,128)(2,1)} custom-call(bf16[768,1024]{1,0:T(8,128)(2,1)} %fusion.pre_ref, f32[3,1024]{1,0:T(4,128)} %taps_ref.7, f32[1,1024]{1,0:T(1,128)} %bitcast.33, bf16[768,1024]{1,0:T(8,128)(2,1)} %forward_mix.2.refs_0_), custom_call_target="tpu_custom_call", output_to_operand_aliasing={{}: (3, {})} | custom-call | tf_op jit(solution)/shard_map/forward_mix/pallas_call | solution.py:146
  195.9 7.3 %collective-permute-done.6 = bf16[96,2048]{1,0:T(8,128)(2,1)S(1)} collective-permute-done((bf16[96,2048]{1,0:T(8,128)(2,1)}, bf16[96,2048]{1,0:T(8,128)(2,1)S(1)}, u32[]{:S(2)}, u32[]{:S(2)}) %collective-permute-start.6) | collective-permute-done | bytes 393248 | tf_op jit(solution)/shard_map/ppermute | solution.py:27
  207.9 2.6 %reduce-scatter.5.cloned.1.call-done.refs_0_ = bf16[256,1024]{1,0:T(8,128)(2,1)} async-done(((bf16[2048,1024]{1,0:T(8,128)(2,1)}), bf16[256,1024]{1,0:T(8,128)(2,1)}) %reduce-scatter.5.cloned.1.call-update) | async-done | bytes 524304 | tf_op jit(solution)/shard_map/reduce_scatter | solution.py:235
  210.5 3.5 %add_terms.3 = (f32[256,1024]{1,0:T(8,128)}, f32[256,1024]{1,0:T(8,128)}) custom-call(bf16[256,1024]{1,0:T(8,128)(2,1)} %reduce-scatter.5.cloned.1.call-done.refs_0_, f32[256,1024]{1,0:T(8,128)} %refs_1_.3, f32[256,1024]{1,0:T(8,128)} %refs_2_.3, f32[256,1024]{1,0:T(8,128)} %get-tuple-element.38.refs_3_, ...), custom_call_target="tpu_custom_call", output_to_operand_aliasing={{0}: (3, {}), {1}: (4, {})} | custom-call | tf_op jit(solution)/shard_map/add_terms/pallas_call | solution.py:172
  214.0 3.2 %collective-permute-done.5 = bf16[192,2048]{1,0:T(8,128)(2,1)} collective-permute-done((bf16[192,2048]{1,0:T(8,128)(2,1)}, bf16[192,2048]{1,0:T(8,128)(2,1)}, u32[]{:S(2)}, u32[]{:S(2)}) %collective-permute-start.5) | collective-permute-done | bytes 786464 | tf_op jit(solution)/shard_map/ppermute | solution.py:27
  217.2 1.6 broadcast_select_fusion.3
  221.5 1.8 pad_maximum_fusion
  (70 shorter events, 23.9 us)
Async XLA Ops:
  7.2 53.1 %copy-start = (bf16[768,2048]{1,0:T(8,128)(2,1)S(1)}, bf16[768,2048]{1,0:T(8,128)(2,1)}, u32[]{:S(2)}) copy-start(bf16[768,2048]{1,0:T(8,128)(2,1)} %param.12) | copy-start | bytes 9437188
  7.2 53.1 %all-gather.5.cloned.1.call-start = ((), (), s32[]{:S(2)}) async-start(), calls=%async_computation.3 | async-start | bytes 4718592 | tf_op jit(solution)/shard_map/all_gather | solution.py:229
  10.5 97.6 %all-gather.3.cloned.1.call-start = ((), (), s32[]{:S(2)}) async-start(), calls=%async_computation.2 | async-start | bytes 4718592 | tf_op jit(solution)/shard_map/all_gather | solution.py:229
  13.7 159.8 %reduce-scatter.3.cloned.1.call-start = ((), (), s32[]{:S(2)}) async-start(), calls=%async_computation.4 | async-start | bytes 4718592 | tf_op jit(solution)/shard_map/reduce_scatter | solution.py:235
  78.4 132.1 %reduce-scatter.5.cloned.1.call-start = ((), (), s32[]{:S(2)}) async-start(), calls=%async_computation.5 | async-start | bytes 4718592 | tf_op jit(solution)/shard_map/reduce_scatter | solution.py:235
  119.7 6.6 %copy-start.12 = (bf16[2048,1024]{1,0:T(8,128)(2,1)S(1)}, bf16[2048,1024]{1,0:T(8,128)(2,1)}, u32[]{:S(2)}) copy-start(bf16[2048,1024]{1,0:T(8,128)(2,1)} %all-gather.3.cloned.1.call-done) | copy-start | bytes 12582916
  119.7 6.6 %copy-start.13 = (bf16[768,1024]{1,0:T(8,128)(2,1)S(1)}, bf16[768,1024]{1,0:T(8,128)(2,1)}, u32[]{:S(2)}) copy-start(bf16[768,1024]{1,0:T(8,128)(2,1)} %get-tuple-element.37) | copy-start | bytes 4718596
  136.4 7.3 %copy-start.9 = (f32[4,512]{1,0:T(4,128)S(1)}, f32[4,512]{1,0:T(4,128)}, u32[]{:S(2)}) copy-start(f32[4,512]{1,0:T(4,128)} %get-tuple-element.42) | copy-start | bytes 24580
  136.4 7.3 %copy-start.10 = (f32[4,512]{1,0:T(4,128)S(1)}, f32[4,512]{1,0:T(4,128)}, u32[]{:S(2)}) copy-start(f32[4,512]{1,0:T(4,128)} %get-tuple-element.43) | copy-start | bytes 24580
  138.6 20.0 %collective-permute-start.2 = (bf16[192,2048]{1,0:T(8,128)(2,1)}, bf16[192,2048]{1,0:T(8,128)(2,1)}, u32[]{:S(2)}, u32[]{:S(2)}) collective-permute-start(bf16[192,2048]{1,0:T(8,128)(2,1)} %constant_dynamic-slice_fusion), channel_id=1, source_target_pairs={{0,2},{1,3},{2,0},{3,1},{4,6},{5,7},{6,4},{7,5},{8,10},{9,11},{10,... | collective-permute-start | bytes 2359304 | tf_op jit(solution)/shard_map/ppermute | solution.py:27
  142.3 19.6 %collective-permute-start = (bf16[192,2048]{1,0:T(8,128)(2,1)}, bf16[192,2048]{1,0:T(8,128)(2,1)}, u32[]{:S(2)}, u32[]{:S(2)}) collective-permute-start(bf16[192,2048]{1,0:T(8,128)(2,1)} %constant_dynamic-slice_fusion.1), channel_id=1, source_target_pairs={{0,1},{1,0},{2,3},{3,2},{4,5},{5,4},{6,7},{7,6},{8,9},{9,8},{10,11... | collective-permute-start | bytes 2359304 | tf_op jit(solution)/shard_map/ppermute | solution.py:27
  143.7 1.2 collective-permute-start.8
  145.0 4.3 %collective-permute-start.9 = (f32[4,1024]{1,0:T(4,128)S(1)}, f32[4,1024]{1,0:T(4,128)S(1)}, u32[]{:S(2)}, u32[]{:S(2)}) collective-permute-start(f32[4,1024]{1,0:T(4,128)S(1)} %add.92), channel_id=1, source_target_pairs={{0,8},{4,12},{8,0},{12,4},{16,24},{20,28},{24,16},{28,20},{1,9},{5... | collective-permute-start | bytes 49160 | tf_op jit(solution)/shard_map/ppermute | solution.py:27
  145.1 16.8 %copy-start.7 = (bf16[384,2048]{1,0:T(8,128)(2,1)S(1)}, bf16[384,2048]{1,0:T(8,128)(2,1)}, u32[]{:S(2)}) copy-start(bf16[384,2048]{1,0:T(8,128)(2,1)} %add_convert_fusion.1) | copy-start | bytes 4718596
  149.3 41.0 %collective-permute-start.10 = (f32[4,1024]{1,0:T(4,128)S(1)}, f32[4,1024]{1,0:T(4,128)}, u32[]{:S(2)}, u32[]{:S(2)}) collective-permute-start(f32[4,1024]{1,0:T(4,128)S(1)} %add.93), channel_id=1, source_target_pairs={{0,16},{4,20},{8,24},{12,28},{16,0},{20,4},{24,8},{28,12},{1,17},{... | collective-permute-start | bytes 49160 | tf_op jit(solution)/shard_map/ppermute | solution.py:27
  160.2 10.4 %collective-permute-start.3 = (bf16[96,2048]{1,0:T(8,128)(2,1)S(1)}, bf16[96,2048]{1,0:T(8,128)(2,1)S(1)}, u32[]{:S(2)}, u32[]{:S(2)}) collective-permute-start(bf16[96,2048]{1,0:T(8,128)(2,1)S(1)} %dynamic-slice_convert_fusion), channel_id=1, source_target_pairs={{0,1},{1,0},{2,3},{3,2},{4,5},{5,4},{6,7},{7,6},{8,9},{9,8},{10,11... | collective-permute-start | bytes 1179656 | tf_op jit(solution)/shard_map/ppermute | solution.py:27
  163.3 10.1 %collective-permute-start.1 = (bf16[96,2048]{1,0:T(8,128)(2,1)S(1)}, bf16[96,2048]{1,0:T(8,128)(2,1)S(1)}, u32[]{:S(2)}, u32[]{:S(2)}) collective-permute-start(bf16[96,2048]{1,0:T(8,128)(2,1)S(1)} %dynamic-slice_convert_fusion.1), channel_id=1, source_target_pairs={{0,2},{1,3},{2,0},{3,1},{4,6},{5,7},{6,4},{7,5},{8,10},{9,11},{10,... | collective-permute-start | bytes 1179656 | tf_op jit(solution)/shard_map/ppermute | solution.py:27
  173.5 12.9 %copy-start.6 = (bf16[96,2048]{1,0:T(8,128)(2,1)}, bf16[96,2048]{1,0:T(8,128)(2,1)S(1)}, u32[]{:S(2)}) copy-start(bf16[96,2048]{1,0:T(8,128)(2,1)S(1)} %add_convert_fusion.3) | copy-start | bytes 1179652
  177.2 14.4 %collective-permute-start.4 = (bf16[96,2048]{1,0:T(8,128)(2,1)S(1)}, bf16[96,2048]{1,0:T(8,128)(2,1)}, u32[]{:S(2)}, u32[]{:S(2)}) collective-permute-start(bf16[96,2048]{1,0:T(8,128)(2,1)S(1)} %add_convert_fusion.3), channel_id=1, source_target_pairs={{0,2},{1,3},{2,0},{3,1},{4,6},{5,7},{6,4},{7,5},{8,10},{9,11},{10,... | collective-permute-start | bytes 1179656 | tf_op jit(solution)/shard_map/ppermute | solution.py:27
  191.0 15.7 %copy-start.11 = (f32[1024]{0:T(1024)S(1)}, f32[1024]{0:T(1024)}, u32[]{:S(2)}) copy-start(f32[1024]{0:T(1024)} %param.21) | copy-start | bytes 12292
  191.0 16.3 %copy-start.8 = (f32[3,1024]{1,0:T(4,128)S(1)}, f32[3,1024]{1,0:T(4,128)}, u32[]{:S(2)}) copy-start(f32[3,1024]{1,0:T(4,128)} %param.20) | copy-start | bytes 36868
  191.0 12.3 %collective-permute-start.6 = (bf16[96,2048]{1,0:T(8,128)(2,1)}, bf16[96,2048]{1,0:T(8,128)(2,1)S(1)}, u32[]{:S(2)}, u32[]{:S(2)}) collective-permute-start(bf16[96,2048]{1,0:T(8,128)(2,1)} %add_convert_fusion.2), channel_id=1, source_target_pairs={{0,1},{1,0},{2,3},{3,2},{4,5},{5,4},{6,7},{7,6},{8,9},{9,8},{10,11... | collective-permute-start | bytes 1179656 | tf_op jit(solution)/shard_map/ppermute | solution.py:27
  192.8 0.8 copy-start.1
  194.5 22.7 %collective-permute-start.5 = (bf16[192,2048]{1,0:T(8,128)(2,1)}, bf16[192,2048]{1,0:T(8,128)(2,1)}, u32[]{:S(2)}, u32[]{:S(2)}) collective-permute-start(bf16[192,2048]{1,0:T(8,128)(2,1)} %pad_maximum_fusion.1), channel_id=1, source_target_pairs={{0,1},{1,0},{2,3},{3,2},{4,5},{5,4},{6,7},{7,6},{8,9},{9,8},{10,11... | collective-permute-start | bytes 2359304 | tf_op jit(solution)/shard_map/ppermute | solution.py:27
  204.3 0.8 copy-start.2
  204.3 1.7 copy-start.4
  206.0 14.0 %collective-permute-start.7 = (bf16[192,2048]{1,0:T(8,128)(2,1)}, bf16[192,2048]{1,0:T(8,128)(2,1)}, u32[]{:S(2)}, u32[]{:S(2)}) collective-permute-start(bf16[192,2048]{1,0:T(8,128)(2,1)} %pad_maximum_fusion.2), channel_id=1, source_target_pairs={{0,2},{1,3},{2,0},{3,1},{4,6},{5,7},{6,4},{7,5},{8,10},{9,11},{10,... | collective-permute-start | bytes 2359304 | tf_op jit(solution)/shard_map/ppermute | solution.py:27
  214.0 6.0 %copy-start.3 = (bf16[96,2048]{1,0:T(8,128)(2,1)S(1)}, bf16[96,2048]{1,0:T(8,128)(2,1)}, u32[]{:S(2)}) copy-start(bf16[96,2048]{1,0:T(8,128)(2,1)} %copy-done.2) | copy-start | bytes 1179652
  214.0 6.0 %copy-start.5 = (bf16[96,2048]{1,0:T(8,128)(2,1)S(1)}, bf16[96,2048]{1,0:T(8,128)(2,1)}, u32[]{:S(2)}) copy-start(bf16[96,2048]{1,0:T(8,128)(2,1)} %copy-done.4) | copy-start | bytes 1179652
Sparse Core Ops, SparseCore 0:
  10.6 49.5 all-gather.4
  62.4 45.6 all-gather.2
  110.5 49.4 reduce-scatter.2
  162.1 48.3 reduce-scatter.4
